TPU v7x, 32 devices: a whole 2x2x4 slice. The times are simulated.
32 devices in a mesh: sp: 16 (over z, y, x), tp: 2 (over core).
Axes of the slice: x: 2, y: 2, z: 4, core: 2. Of those that a mesh axis runs over, the one named last changes fastest.
Arguments:
- tokens: bfloat16 [4096, 2048], P('sp', 'tp'), may hold values from -6 to 6
- norm_gain: float32 [2048], replicated, may hold values from 0.1 to 1.9
- query_weight: bfloat16 [1024, 2048], P('tp'), may hold values from -0.125 to 0.125
- key_weight: bfloat16 [1024, 2048], P('tp'), may hold values from -0.125 to 0.125
- value_weight: bfloat16 [1024, 2048], P('tp'), may hold values from -0.125 to 0.125
- pool_weight: bfloat16 [1024, 2048], P('tp'), may hold values from -0.125 to 0.125
- query_gain: float32 [64], replicated, may hold values from 0.6 to 6
- key_gain: float32 [64], replicated, may hold values from 0.6 to 6
- cum_gate: float32 [4096, 16], P('sp', 'tp'), as said below
- out_pool_weight: bfloat16 [1024, 2048], P(None, 'tp'), may hold values from -0.1875 to 0.1875
- out_attn_weight: bfloat16 [1024, 2048], P(None, 'tp'), may hold values from -0.1875 to 0.1875
Outputs:
- mixed: bfloat16 [4096, 2048], P('sp', 'tp')
Inputs may be any that keep to these rules, and one draw needn't show every extreme that they name: `cum_gate`: in each head the values never rise along the positions.
All inputs are finite; a program needn't handle non-finite values.
Results may differ from a plain program's by a relative error of at most 0.005.
The roundings to bfloat16 on the way count: a program that leaves them out, or rounds other values in their place, can miss the bound.
Values may be sent and summed in bfloat16 or wider, within the bound.
A program may use at most 128 MiB of HBM per device.

v0:
```python
import math
import jax
import jax.numpy as jnp
from jax import lax
from jax.sharding import PartitionSpec as P

HEAD_DIM = 64
POOL_WIDTH = 1024
POOL_GROUPS = 4
epsilon = 1e-06
masked_fill = -1e30


def from_behind(value, axis, steps):
    count = lax.axis_size(axis)
    leading, last = (max(0, -steps), min(count, count - steps))
    return lax.ppermute(value, axis, [(source, source + steps) for source in range(leading, last)])


def rms_scale(values, gain):
    return values * lax.rsqrt(jnp.mean(values * values, axis=-1, keepdims=True) + epsilon) * gain


def block_partials(query_rows, query_pos, query_gate, key_rows, value_rows, key_pos, key_gate):
    logits = jnp.einsum("qhd,gkhd->qhgk", query_rows, key_rows, preferred_element_type=jnp.float32)
    logits = logits + query_gate[:, :, None, None] - jnp.transpose(key_gate, (2, 0, 1))[None]
    allowed = key_pos[None, None, :, :] <= query_pos[:, None, None, None]
    logits = jnp.where(allowed, logits, masked_fill)
    block_max = jnp.max(logits, axis=-1)
    weights = jnp.where(allowed, jnp.exp(logits - block_max[..., None]), 0.0)
    totals = jnp.sum(weights, axis=-1)
    numerator = jnp.einsum(
        "qhgk,gkhd->qhgd",
        weights.astype(jnp.bfloat16),
        value_rows,
        preferred_element_type=jnp.float32,
    )
    return (block_max, totals, numerator)


def merge_state(state, partials):
    run_max, run_den, run_acc = state
    block_max, totals, numerator = partials
    new_max = jnp.maximum(run_max, jnp.max(block_max, axis=-1))
    old_scale = jnp.exp(run_max - new_max)
    block_scale = jnp.exp(block_max - new_max[..., None])
    new_den = run_den * old_scale + jnp.sum(block_scale * totals, axis=-1)
    new_acc = run_acc * old_scale[..., None] + jnp.sum(block_scale[..., None] * numerator, axis=2)
    return (new_max, new_den, new_acc)


def empty_state(rows, heads_here):
    return (
        jnp.full((rows, heads_here), masked_fill, jnp.float32),
        jnp.zeros((rows, heads_here), jnp.float32),
        jnp.zeros((rows, heads_here, HEAD_DIM), jnp.float32),
    )


def per_device(
    tokens,
    norm_gain,
    query_weight,
    key_weight,
    value_weight,
    pool_weight,
    query_gain,
    key_gain,
    cum_gate,
    out_pool_weight,
    out_attn_weight,
):
    full_rows = lax.all_gather(tokens, "tp", axis=1, tiled=True)
    normed = rms_scale(full_rows.astype(jnp.float32), norm_gain).astype(jnp.bfloat16)
    length = full_rows.shape[0]
    heads_here = cum_gate.shape[1]
    offset = lax.axis_index("sp") * length

    def project(weight):
        return lax.dot_general(
            normed, weight, (((1,), (1,)), ((), ())), preferred_element_type=jnp.float32
        )

    query_heads = (
        rms_scale(project(query_weight).reshape(length, heads_here, HEAD_DIM), query_gain)
        * HEAD_DIM ** (-0.5)
    ).astype(jnp.bfloat16)
    key_heads = rms_scale(
        project(key_weight).reshape(length, heads_here, HEAD_DIM), key_gain
    ).astype(jnp.bfloat16)
    value_heads = project(value_weight).astype(jnp.bfloat16).reshape(length, heads_here, HEAD_DIM)
    pool_input = project(pool_weight).astype(jnp.bfloat16)
    reach = 2**POOL_GROUPS
    rim_rows = from_behind(pool_input[length - reach :], "sp", 1)
    extended = jnp.concatenate([rim_rows, pool_input], axis=0).astype(jnp.float32)
    prefix = jnp.cumsum(extended, axis=0)
    width_here = pool_input.shape[1]
    channel_ids = lax.axis_index("tp") * width_here + jnp.arange(width_here, dtype=jnp.int32)
    group_ids = channel_ids // (POOL_WIDTH // POOL_GROUPS)
    counts = (offset + jnp.arange(1, length + 1, dtype=jnp.int32)).astype(jnp.float32)[:, None]
    current = prefix[reach:]
    pooled_mean = jnp.zeros((length, width_here), jnp.float32)
    for group_index in range(POOL_GROUPS):
        window = 2 ** (group_index + 1)
        lagged = prefix[reach - window : reach - window + length]
        average = (current - lagged) / jnp.minimum(counts, float(window))
        pooled_mean = jnp.where(group_ids[None, :] == group_index, average, pooled_mean)
    pooled = (pooled_mean - extended[reach:]).astype(jnp.bfloat16)
    gate_all = lax.all_gather(cum_gate, "sp", axis=0, tiled=True)
    query_pos = offset + jnp.arange(length, dtype=jnp.int32)
    key_flat = key_heads.reshape(length, heads_here * HEAD_DIM)
    value_flat = value_heads.reshape(length, heads_here * HEAD_DIM)

    def absorb(carried, inputs):
        key_rows, value_rows, key_gate, key_pos = inputs
        partials = block_partials(
            query_heads, query_pos, cum_gate, key_rows, value_rows, key_pos, key_gate
        )
        return (merge_state(carried, partials), None)

    key_piece = lax.all_gather(key_flat, "sp", axis=0, tiled=True)
    value_piece = lax.all_gather(value_flat, "sp", axis=0, tiled=True)
    shards = key_piece.shape[0] // length
    grouping = math.gcd(shards, 8)
    turns = shards // grouping
    key_groups = key_piece.reshape(turns, grouping, length, heads_here, HEAD_DIM)
    value_groups = value_piece.reshape(turns, grouping, length, heads_here, HEAD_DIM)
    gate_groups = gate_all.reshape(turns, grouping, length, heads_here)
    pos_groups = jnp.arange(shards * length, dtype=jnp.int32).reshape(turns, grouping, length)
    result, _ = lax.scan(
        absorb, empty_state(length, heads_here), (key_groups, value_groups, gate_groups, pos_groups)
    )
    final_max, final_den, final_acc = result
    attended = (
        (final_acc / final_den[..., None])
        .reshape(length, heads_here * HEAD_DIM)
        .astype(jnp.bfloat16)
    )
    pool_full, attn_full = (
        lax.all_gather(pooled, "tp", axis=1, tiled=True),
        lax.all_gather(attended, "tp", axis=1, tiled=True),
    )
    output = jnp.dot(pool_full, out_pool_weight, preferred_element_type=jnp.float32) + jnp.dot(
        attn_full, out_attn_weight, preferred_element_type=jnp.float32
    )
    return output.astype(jnp.bfloat16)


def solution(mesh):
    return jax.shard_map(
        per_device,
        mesh=mesh,
        in_specs=(
            P("sp", "tp"),
            P(),
            P("tp", None),
            P("tp", None),
            P("tp", None),
            P("tp", None),
            P(),
            P(),
            P("sp", "tp"),
            P(None, "tp"),
            P(None, "tp"),
        ),
        out_specs=P("sp", "tp"),
        check_vma=False,
    )
```

profile of v0, /device:TPU:0, one launch (start us, length us, event | category | flops | bytes accessed | tf_op | source)
XLA Modules:
  0.0 260.2 jit_solution(4839599759511507353)
XLA Ops:
  6.5 0.7 all-gather.4.cloned.1.call-update
  7.3 0.7 mul.114
  8.0 12.6 %all-gather.4.cloned.1.call-done = bf16[256,2048]{1,0:T(8,128)(2,1)} async-done(((bf16[256,1024]{1,0:T(8,128)(2,1)}), bf16[256,2048]{1,0:T(8,128)(2,1)}) %all-gather.4.cloned.1.call-update) | async-done | bytes 1048592 | tf_op jit(solution)/shard_map/all_gather | solution.py:73
  20.7 1.5 fusion.24
  22.2 2.8 %fusion.50 = (f32[256,512]{1,0:T(8,128)S(1)}, f32[256,512]{1,0:T(8,128)}) fusion(bf16[512,2048]{1,0:T(8,128)(2,1)S(1)} %copy-done, bf16[256,2048]{1,0:T(8,128)(2,1)} %all-gather.4.cloned.1.call-done, f32[2048]{0:T(1024)} %param.14, f32[256]{0:T(256)S(1)} %add_rsqrt_fusion.2), kind=kOutput, calls=%fused_computation.93 | convolution fusion | flops 539099136 | bytes 4203520 | tf_op jit(solution)/shard_map/dot_general | solution.py:80
  26.0 0.8 multiply_convert_fusion.1
  26.9 3.0 %convolution_convert_fusion = bf16[256,512]{1,0:T(8,128)(2,1)} fusion(bf16[512,2048]{1,0:T(8,128)(2,1)} %param.17, bf16[256,2048]{1,0:T(8,128)(2,1)S(1)} %copy-done.4, f32[2048]{0:T(1024)S(1)} %copy-done.9, f32[256]{0:T(256)S(1)} %add_rsqrt_fusion.2), kind=kOutput, calls=%fused_computation.41 | convolution fusion | flops 539099136 | bytes 3417088 | tf_op jit(solution)/shard_map/dot_general | solution.py:80
  30.0 42.8 %all_gather.21 = f32[4096,8]{0,1:T(8,128)S(1)} all-gather(f32[256,8]{0,1:T(8,128)S(1)} %copy-done.6), channel_id=1, replica_groups=mesh['sp'=16,'tp'=2] {'sp'}, dimensions={0}, use_global_device_ids=true | all-gather | bytes 139264 | tf_op jit(solution)/shard_map/all_gather | solution.py:109
  72.9 2.5 convolution_convert_fusion.1
  75.4 1.3 collective-permute-start
  76.7 0.8 multiply_reduce_fusion.1
  77.7 0.7 collective-permute-done
  78.6 0.5 fusion.28
  80.2 2.5 all_gather.19
  82.7 0.7 fusion.51
  83.4 20.9 %all-gather.6.cloned.1.call-done = bf16[4096,512]{1,0:T(8,128)(2,1)} async-done(((bf16[256,512]{1,0:T(8,128)(2,1)}), bf16[4096,512]{1,0:T(8,128)(2,1)}) %all-gather.6.cloned.1.call-update) | async-done | bytes 4194320 | tf_op jit(solution)/shard_map/all_gather | solution.py:121
  104.3 11.2 %reshape.154 = bf16[2,8,256,8,64]{4,3,2,1,0:T(8,128)(2,1)} reshape(bf16[4096,512]{1,0:T(8,128)(2,1)} %all-gather.6.cloned.1.call-done) | data formatting | bytes 8388608 | tf_op jit(solution)/shard_map/reshape | solution.py:126
  115.5 9.8 %copy.42 = bf16[2,8,256,8,64]{2,4,1,3,0:T(8,128)(2,1)} copy(bf16[2,8,256,8,64]{4,3,2,1,0:T(8,128)(2,1)} %reshape.154) | data formatting | bytes 8388608
  125.3 56.0 %all-gather.8.cloned.1.call-done = bf16[4096,512]{1,0:T(8,128)(2,1)} async-done(((bf16[256,512]{1,0:T(8,128)(2,1)}), bf16[4096,512]{1,0:T(8,128)(2,1)}) %all-gather.8.cloned.1.call-update) | async-done | bytes 4194320 | tf_op jit(solution)/shard_map/all_gather | solution.py:122
  181.3 11.2 %reshape.155 = bf16[2,8,256,8,64]{4,3,2,1,0:T(8,128)(2,1)} reshape(bf16[4096,512]{1,0:T(8,128)(2,1)} %all-gather.8.cloned.1.call-done) | data formatting | bytes 8388608 | tf_op jit(solution)/shard_map/reshape | solution.py:127
  192.5 9.8 %copy.44 = bf16[2,8,256,8,64]{2,4,1,3,0:T(8,128)(2,1)} copy(bf16[2,8,256,8,64]{4,3,2,1,0:T(8,128)(2,1)} %reshape.155) | data formatting | bytes 8388608
  202.2 46.0 %while.15 = (s32[]{:T(128)}, f32[256,8]{0,1:T(8,128)S(1)}, f32[256,8]{0,1:T(8,128)S(1)}, f32[256,8,64]{0,2,1:T(8,128)S(1)}, s32[2,8,256]{2,1,0:T(8,128)S(1)}, /*...) while((s32[]{:T(128)}, f32[256,8]{0,1:T(8,128)S(1)}, ...), condition=%wide.region_11.12_spmd.clone, body=%wide.region_5.11_spmd.clone.sunk | while | flops 1122789632 | bytes 127101120 | solution.py:130
  202.8 6.9 %fusion.69 = (f32[256,8,8]{0,2,1:T(8,128)S(1)}, f32[256,8,8,256]{0,3,2,1:T(8,128)S(1)}) fusion(f32[8,8,256]{2,1,0:T(8,128)S(1)} %bitcast.72, f32[256,8]{0,1:T(8,128)S(1)} %get-tuple-element.297, bf16[256,8,64]{0,2,1:T(8,128)(2,1)S(1)} %get-tuple-element.296, bf16[2,8,256,8,64]{2,4,1,3,0:T(8,128)(2,1)} %get-tuple-element.295, s32[]{:T(128)S(6)} %copy.63, ...), kind=kOutput, calls=%fused_computation.92.clone.1 | convolution fusion | flops 553631744 | bytes 19800068 | tf_op jit(solution)/shard_map/while/body/eval_jaxpr/qhd,gkhd->qhgk/dot_general | solution.py:25
  209.7 4.8 %fusion.70 = (f32[256,8,8]{0,2,1:T(8,128)S(1)}, f32[256,8]{0,1:T(8,128)S(1)}) fusion(f32[256,8,8,256]{0,3,2,1:T(8,128)S(1)} %get-tuple-element.256, f32[256,8,8]{0,2,1:T(8,128)S(1)} %get-tuple-element.257, pred[256,8,256]{0,2,1:T(8,128)(4,1)S(1)} %broadcast_compare_fusion.6), kind=kLoop, calls=%fused_computation.6.clone.1 | loop fusion | flops 16758784 | bytes 17440768 | tf_op jit(solution)/shard_map/while/body/eval_jaxpr/reduce_sum | solution.py:31
  214.5 0.9 copy-done.2
  215.5 9.5 %fusion.72 = f32[256,8,64]{0,2,1:T(8,128)S(1)} fusion(f32[256,8,8,256]{0,3,2,1:T(8,128)} %copy-done.2, f32[256,8,8]{0,2,1:T(8,128)S(1)} %get-tuple-element.257, pred[256,8,256]{0,2,1:T(8,128)(4,1)S(1)} %broadcast_compare_fusion.6, bf16[2,8,256,8,64]{2,4,1,3,0:T(8,128)(2,1)} %get-tuple-element.299, s32[]{:T(128)S(6)} %copy.63, ...), kind=kOutput, calls=%fused_computation.12.clone.1 | convolution fusion | flops 551419904 | bytes 20054020 | tf_op jit(solution)/shard_map/while/body/eval_jaxpr/qhgk,gkhd->qhgd/dot_general | solution.py:32
  225.8 6.9 %fusion.69 = (f32[256,8,8]{0,2,1:T(8,128)S(1)}, f32[256,8,8,256]{0,3,2,1:T(8,128)S(1)}) fusion(f32[8,8,256]{2,1,0:T(8,128)S(1)} %bitcast.72, f32[256,8]{0,1:T(8,128)S(1)} %get-tuple-element.297, bf16[256,8,64]{0,2,1:T(8,128)(2,1)S(1)} %get-tuple-element.296, bf16[2,8,256,8,64]{2,4,1,3,0:T(8,128)(2,1)} %get-tuple-element.295, s32[]{:T(128)S(6)} %copy.63, ...), kind=kOutput, calls=%fused_computation.92.clone.1 | convolution fusion | flops 553631744 | bytes 19800068 | tf_op jit(solution)/shard_map/while/body/eval_jaxpr/qhd,gkhd->qhgk/dot_general | solution.py:25
  232.7 4.8 %fusion.70 = (f32[256,8,8]{0,2,1:T(8,128)S(1)}, f32[256,8]{0,1:T(8,128)S(1)}) fusion(f32[256,8,8,256]{0,3,2,1:T(8,128)S(1)} %get-tuple-element.256, f32[256,8,8]{0,2,1:T(8,128)S(1)} %get-tuple-element.257, pred[256,8,256]{0,2,1:T(8,128)(4,1)S(1)} %broadcast_compare_fusion.6), kind=kLoop, calls=%fused_computation.6.clone.1 | loop fusion | flops 16758784 | bytes 17440768 | tf_op jit(solution)/shard_map/while/body/eval_jaxpr/reduce_sum | solution.py:31
  237.5 0.9 copy-done.2
  238.5 9.5 %fusion.72 = f32[256,8,64]{0,2,1:T(8,128)S(1)} fusion(f32[256,8,8,256]{0,3,2,1:T(8,128)} %copy-done.2, f32[256,8,8]{0,2,1:T(8,128)S(1)} %get-tuple-element.257, pred[256,8,256]{0,2,1:T(8,128)(4,1)S(1)} %broadcast_compare_fusion.6, bf16[2,8,256,8,64]{2,4,1,3,0:T(8,128)(2,1)} %get-tuple-element.299, s32[]{:T(128)S(6)} %copy.63, ...), kind=kOutput, calls=%fused_computation.12.clone.1 | convolution fusion | flops 551419904 | bytes 20054020 | tf_op jit(solution)/shard_map/while/body/eval_jaxpr/qhgk,gkhd->qhgd/dot_general | solution.py:32
  248.3 2.3 all_gather.23
  250.6 3.1 %fusion.27 = bf16[256,1024]{1,0:T(8,128)(2,1)} fusion(f32[256,1024]{1,0:T(8,128)S(1)} %fusion.51, bf16[256,1024]{0,1:T(8,128)(2,1)S(1)} %all_gather.23, bf16[1024,1024]{1,0:T(8,128)(2,1)} %param.23), kind=kOutput, calls=%fused_computation.40 | convolution fusion | flops 537395200 | bytes 4194304 | tf_op jit(solution)/shard_map/dot_general | solution.py:143
  (71 shorter events, 4.2 us)
Async XLA Ops:
  6.5 15.6 %copy-start = (bf16[512,2048]{1,0:T(8,128)(2,1)S(1)}, bf16[512,2048]{1,0:T(8,128)(2,1)}, u32[]{:S(2)}) copy-start(bf16[512,2048]{1,0:T(8,128)(2,1)} %param.16) | copy-start | bytes 6291460
  6.5 14.1 %all-gather.4.cloned.1.call-start = ((), (), s32[]{:S(2)}) async-start(), calls=%async_computation | async-start | bytes 1572864 | tf_op jit(solution)/shard_map/all_gather | solution.py:73
  7.3 97.0 %all-gather.6.cloned.1.call-start = ((), (), s32[]{:S(2)}) async-start(), calls=%async_computation.1 | async-start | bytes 4456448 | tf_op jit(solution)/shard_map/all_gather | solution.py:121
  25.0 1.0 copy-start.5
  25.2 1.7 copy-start.4
  25.2 1.7 copy-start.9
  26.8 3.2 %copy-start.6 = (f32[256,8]{0,1:T(8,128)S(1)}, f32[256,8]{0,1:T(8,128)}, u32[]{:S(2)}) copy-start(f32[256,8]{0,1:T(8,128)} %param.21) | copy-start | bytes 24580
  26.9 154.4 %all-gather.8.cloned.1.call-start = ((), (), s32[]{:S(2)}) async-start(), calls=%async_computation.2 | async-start | bytes 4456448 | tf_op jit(solution)/shard_map/all_gather | solution.py:122
  72.9 3.8 %copy-start.8 = (bf16[512,2048]{1,0:T(8,128)(2,1)S(1)}, bf16[512,2048]{1,0:T(8,128)(2,1)}, u32[]{:S(2)}) copy-start(bf16[512,2048]{1,0:T(8,128)(2,1)} %param.15) | copy-start | bytes 6291460
  75.4 2.2 copy-start.7
  75.4 3.0 %collective-permute-start = (bf16[16,512]{1,0:T(8,128)(2,1)S(1)}, bf16[16,512]{1,0:T(8,128)(2,1)S(1)}, u32[]{:S(2)}, u32[]{:S(2)}) collective-permute-start(bf16[16,512]{1,0:T(8,128)(2,1)S(1)} %slice.42), channel_id=1, source_target_pairs={{0,2},{2,4},{4,6},{6,8},{8,10},{10,12},{12,14},{14,16},{16,18},{18... | collective-permute-start | bytes 49160 | tf_op jit(solution)/shard_map/ppermute | solution.py:17
  79.7 3.0 %copy-start.3 = (bf16[1024,1024]{1,0:T(8,128)(2,1)S(1)}, bf16[1024,1024]{1,0:T(8,128)(2,1)}, u32[]{:S(2)}) copy-start(bf16[1024,1024]{1,0:T(8,128)(2,1)} %param.22) | copy-start | bytes 6291460
  209.7 5.7 %copy-start.2 = (f32[256,8,8,256]{0,3,2,1:T(8,128)}, f32[256,8,8,256]{0,3,2,1:T(8,128)S(1)}, u32[]{:S(2)}) copy-start(f32[256,8,8,256]{0,3,2,1:T(8,128)S(1)} %get-tuple-element.256) | copy-start | bytes 50331652 | tf_op jit(solution)/shard_map/while
  232.7 5.7 %copy-start.2 = (f32[256,8,8,256]{0,3,2,1:T(8,128)}, f32[256,8,8,256]{0,3,2,1:T(8,128)S(1)}, u32[]{:S(2)}) copy-start(f32[256,8,8,256]{0,3,2,1:T(8,128)S(1)} %get-tuple-element.256) | copy-start | bytes 50331652 | tf_op jit(solution)/shard_map/while
  248.2 5.4 %copy-start.1 = (bf16[512,2048]{1,0:T(8,128)(2,1)S(1)}, bf16[512,2048]{1,0:T(8,128)(2,1)}, u32[]{:S(2)}) copy-start(bf16[512,2048]{1,0:T(8,128)(2,1)} %param.16) | copy-start | bytes 6291460
Sparse Core Ops, SparseCore 0:
  8.9 11.7 all-gather.3
  27.0 77.2 all-gather.5
  107.1 74.1 all-gather.7
where the time goes:
time: 262 us; the launch traced here: 260 us
  waiting for transfers between devices  90.9 us (35%)
  blocking collectives  47.6 us (18%)
  local copies, waits for them, and re-layouts  45.9 us (18%)
  matrix products  45.8 us (17%)
  other arithmetic  15 us (6%)
  between operations  13.4 us (5%)
    all_gather x1, waiting for transfers between devices, per_device(): value_piece = lax.all_gather(value_flat, 'sp', axis=0, tiled=True)  56 us
    all_gather x1, blocking collectives, per_device(): gate_all = lax.all_gather(cum_gate, 'sp', axis=0, tiled=True)  42.8 us
    all_gather x1, waiting for transfers between devices, per_device(): key_piece = lax.all_gather(key_flat, 'sp', axis=0, tiled=True)  20.9 us
    unnamed x20, local copies, waits for them, and re-layouts  20.1 us
    dot_general x2, matrix products, block_partials(): jnp.einsum('qhgk,gkhd->qhgd', weights.astype(jnp.bfloat16), value_rows, p...  19 us
    dot_general x2, matrix products, block_partials(): jnp.einsum('qhd,gkhd->qhgk', query_rows, key_rows, preferred_element_type...  13.8 us
    all_gather x1, waiting for transfers between devices, per_device(): full_rows = lax.all_gather(tokens, 'tp', axis=1, tiled=True)  12.6 us
    reshape x1, local copies, waits for them, and re-layouts, per_device(): key_piece.reshape(turns, grouping, length, heads_here, HEAD_DIM)  11.2 us
  transfers between devices with their start and end apart: 4, of which 4 were waited for; matrix products, arithmetic and copies ran while one was open for 12% of the time, Pallas kernels for 0%

commit v1 on v0

--- a/solution.py
+++ b/solution.py
@@ -106,7 +106,6 @@
         average = (current - lagged) / jnp.minimum(counts, float(window))
         pooled_mean = jnp.where(group_ids[None, :] == group_index, average, pooled_mean)
     pooled = (pooled_mean - extended[reach:]).astype(jnp.bfloat16)
-    gate_all = lax.all_gather(cum_gate, "sp", axis=0, tiled=True)
     query_pos = offset + jnp.arange(length, dtype=jnp.int32)
     key_flat = key_heads.reshape(length, heads_here * HEAD_DIM)
     value_flat = value_heads.reshape(length, heads_here * HEAD_DIM)
@@ -118,7 +117,11 @@
         )
         return (merge_state(carried, partials), None)
 
-    key_piece = lax.all_gather(key_flat, "sp", axis=0, tiled=True)
+    gate_all, key_piece = jnp.split(
+        lax.all_gather(jnp.concatenate([cum_gate, key_flat], axis=1), "sp", axis=0, tiled=True),
+        [cum_gate.shape[1]],
+        axis=1,
+    )
     value_piece = lax.all_gather(value_flat, "sp", axis=0, tiled=True)
     shards = key_piece.shape[0] // length
     grouping = math.gcd(shards, 8)

time: 262 us -> 329 us (1.26)
  waiting for transfers between devices: 90.9 us -> 186 us
  blocking collectives: 47.6 us -> 4.81 us
  local copies, waits for them, and re-layouts: 45.9 us -> 58.7 us
    all_gather x1, waiting for transfers between devices: 20.9 us -> 112 us  [per_device(): lax.all_gather(jnp.concatenate([cum_gate, key_flat], axis=1), 'sp', axis=...]
    all_gather x1 -> x0, blocking collectives: 42.8 us -> none  [per_device(): gate_all = lax.all_gather(cum_gate, 'sp', axis=0, tiled=True)]
    split x0 -> x2, local copies, waits for them, and re-layouts: none -> 10.6 us  [per_device(): jnp.split(lax.all_gather(jnp.concatenate([cum_gate, key_flat], axis=1), '...]
    unnamed x20 -> x24, local copies, waits for them, and re-layouts: 20.1 us -> 21.9 us
  transfers between devices with their start and end apart: 4 -> 4, of which waited for: 4 -> 4; matrix products, arithmetic and copies ran while one was open for 12% -> 10% of each run, Pallas kernels for 0% -> 0%
where the time goes in v1:
time: 329 us; the launch traced here: 327 us
  waiting for transfers between devices  186 us (57%)
  local copies, waits for them, and re-layouts  58.7 us (18%)
  matrix products  45.2 us (14%)
  other arithmetic  15.4 us (5%)
  between operations  13.5 us (4%)
  blocking collectives  4.81 us (1%)
  starting transfers between devices  3.72 us (1%)
    all_gather x1, waiting for transfers between devices, per_device(): lax.all_gather(jnp.concatenate([cum_gate, key_flat], axis=1), 'sp', axis=...  112 us
    all_gather x1, waiting for transfers between devices, per_device(): value_piece = lax.all_gather(value_flat, 'sp', axis=0, tiled=True)  59.3 us
    unnamed x24, local copies, waits for them, and re-layouts  21.9 us
    dot_general x2, matrix products, block_partials(): jnp.einsum('qhgk,gkhd->qhgd', weights.astype(jnp.bfloat16), value_rows, p...  19.1 us
    dot_general x2, matrix products, block_partials(): jnp.einsum('qhd,gkhd->qhgk', query_rows, key_rows, preferred_element_type...  13.8 us
    all_gather x1, waiting for transfers between devices, per_device(): full_rows = lax.all_gather(tokens, 'tp', axis=1, tiled=True)  13.4 us
    reshape x1, local copies, waits for them, and re-layouts, per_device(): value_piece.reshape(turns, grouping, length, heads_here, HEAD_DIM)  11.2 us
    reshape x1, local copies, waits for them, and re-layouts, per_device(): key_piece.reshape(turns, grouping, length, heads_here, HEAD_DIM)  11.2 us
  transfers between devices with their start and end apart: 4, of which 4 were waited for; matrix products, arithmetic and copies ran while one was open for 10% of the time, Pallas kernels for 0%

profile of v1, /device:TPU:0, one launch (start us, length us, event | category | flops | bytes accessed | tf_op | source)
XLA Modules:
  0.0 327.1 jit_solution(12159646833383032293)
XLA Ops:
  6.5 0.7 all-gather.4.cloned.1.call-update
  7.3 13.4 %all-gather.4.cloned.1.call-done = bf16[256,2048]{1,0:T(8,128)(2,1)} async-done(((bf16[256,1024]{1,0:T(8,128)(2,1)}), bf16[256,2048]{1,0:T(8,128)(2,1)}) %all-gather.4.cloned.1.call-update) | async-done | bytes 1048592 | tf_op jit(solution)/shard_map/all_gather | solution.py:73
  20.7 1.5 fusion.24
  22.2 3.5 %convolution_convert_fusion = bf16[256,512]{1,0:T(8,128)(2,1)} fusion(bf16[512,2048]{1,0:T(8,128)(2,1)} %param.17, bf16[256,2048]{1,0:T(8,128)(2,1)} %all-gather.4.cloned.1.call-done, f32[2048]{0:T(1024)} %param.14, f32[256]{0:T(256)S(1)} %add_rsqrt_fusion.2), kind=kOutput, calls=%fused_computation.40 | convolution fusion | flops 539099136 | bytes 3417088 | tf_op jit(solution)/shard_map/dot_general | solution.py:80
  26.0 1.7 fusion.51
  27.8 1.3 copy.40
  29.5 1.1 pad_maximum_fusion
  30.7 2.5 convolution_convert_fusion.1
  33.3 3.6 %collective-permute-start = (bf16[16,512]{1,0:T(8,128)(2,1)S(1)}, bf16[16,512]{1,0:T(8,128)(2,1)S(1)}, u32[]{:S(2)}, u32[]{:S(2)}) collective-permute-start(bf16[16,512]{1,0:T(8,128)(2,1)S(1)} %slice.42), channel_id=1, source_target_pairs={{0,2},{2,4},{4,6},{6,8},{8,10},{10,12},{12,14},{14,16},{16,18},{18... | collective-permute-start | bytes 49160 | tf_op jit(solution)/shard_map/ppermute | solution.py:17
  36.9 0.8 multiply_reduce_fusion.1
  40.2 2.5 all_gather.16
  42.7 0.7 fusion.52
  43.4 59.3 %all-gather.8.cloned.1.call-done = bf16[4096,512]{1,0:T(8,128)(2,1)} async-done(((bf16[256,512]{1,0:T(8,128)(2,1)}), bf16[4096,512]{1,0:T(8,128)(2,1)}) %all-gather.8.cloned.1.call-update) | async-done | bytes 4194320 | tf_op jit(solution)/shard_map/all_gather | solution.py:125
  102.7 11.2 %reshape.155 = bf16[2,8,256,8,64]{4,3,2,1,0:T(8,128)(2,1)} reshape(bf16[4096,512]{1,0:T(8,128)(2,1)} %all-gather.8.cloned.1.call-done) | data formatting | bytes 8388608 | tf_op jit(solution)/shard_map/reshape | solution.py:130
  113.9 9.8 %copy.48 = bf16[2,8,256,8,64]{2,4,1,3,0:T(8,128)(2,1)} copy(bf16[2,8,256,8,64]{4,3,2,1,0:T(8,128)(2,1)} %reshape.155) | data formatting | bytes 8388608
  123.7 111.8 %all-gather.6.cloned.1.call-done = f32[4096,520]{1,0:T(8,128)} async-done(((f32[256,520]{1,0:T(8,128)}), f32[4096,520]{1,0:T(8,128)}) %all-gather.6.cloned.1.call-update) | async-done | bytes 8519696 | tf_op jit(solution)/shard_map/all_gather | solution.py:121
  235.5 7.5 %split.8 = bf16[4096,512]{1,0:T(8,128)(2,1)} slice(f32[4096,520]{1,0:T(8,128)} %all-gather.6.cloned.1.call-done), slice={[0:4096], [8:520]} | slice | bytes 8388608 | tf_op jit(solution)/shard_map/split | solution.py:120
  243.0 11.2 %reshape.154 = bf16[2,8,256,8,64]{4,3,2,1,0:T(8,128)(2,1)} reshape(bf16[4096,512]{1,0:T(8,128)(2,1)} %split.8) | data formatting | bytes 8388608 | tf_op jit(solution)/shard_map/reshape | solution.py:129
  254.2 9.8 %copy.46 = bf16[2,8,256,8,64]{2,4,1,3,0:T(8,128)(2,1)} copy(bf16[2,8,256,8,64]{4,3,2,1,0:T(8,128)(2,1)} %reshape.154) | data formatting | bytes 8388608
  263.9 3.0 split.9
  267.0 2.1 copy.47
  269.1 46.0 %while.15 = (s32[]{:T(128)}, f32[256,8]{0,1:T(8,128)S(1)}, f32[256,8]{0,1:T(8,128)S(1)}, f32[256,8,64]{0,2,1:T(8,128)S(1)}, s32[2,8,256]{2,1,0:T(8,128)S(1)}, /*...) while((s32[]{:T(128)}, f32[256,8]{0,1:T(8,128)S(1)}, ...), condition=%wide.region_11.12_spmd.clone, body=%wide.region_5.11_spmd.clone.sunk | while | flops 1122789632 | bytes 126970048 | solution.py:133
  269.7 6.9 %fusion.70 = (f32[256,8,8]{0,2,1:T(8,128)S(1)}, f32[256,8,8,256]{0,3,2,1:T(8,128)S(1)}) fusion(f32[8,8,256]{2,1,0:T(8,128)S(1)} %dynamic-slice_bitcast_fusion.4, f32[256,8]{0,1:T(8,128)S(1)} %get-tuple-element.297, bf16[256,8,64]{0,2,1:T(8,128)(2,1)S(1)} %get-tuple-element.296, bf16[2,8,256,8,64]{2,4,1,3,0:T(8,128)(2,1)} %get-tuple-element.295, ...), kind=kOutput, calls=%fused_computation.93.clone.1 | convolution fusion | flops 553631744 | bytes 19800068 | tf_op jit(solution)/shard_map/while/body/eval_jaxpr/qhd,gkhd->qhgk/dot_general | solution.py:25
  276.6 4.8 %fusion.71 = (f32[256,8,8]{0,2,1:T(8,128)S(1)}, f32[256,8]{0,1:T(8,128)S(1)}) fusion(f32[256,8,8,256]{0,3,2,1:T(8,128)S(1)} %get-tuple-element.256, f32[256,8,8]{0,2,1:T(8,128)S(1)} %get-tuple-element.257, pred[256,8,256]{0,2,1:T(8,128)(4,1)S(1)} %broadcast_compare_fusion.6), kind=kLoop, calls=%fused_computation.6.clone.1 | loop fusion | flops 16758784 | bytes 17440768 | tf_op jit(solution)/shard_map/while/body/eval_jaxpr/reduce_sum | solution.py:31
  281.4 0.9 copy-done.2
  282.4 9.5 %fusion.73 = f32[256,8,64]{0,2,1:T(8,128)S(1)} fusion(f32[256,8,8,256]{0,3,2,1:T(8,128)} %copy-done.2, f32[256,8,8]{0,2,1:T(8,128)S(1)} %get-tuple-element.257, pred[256,8,256]{0,2,1:T(8,128)(4,1)S(1)} %broadcast_compare_fusion.6, bf16[2,8,256,8,64]{2,4,1,3,0:T(8,128)(2,1)} %get-tuple-element.299, s32[]{:T(128)S(6)} %copy.62, ...), kind=kOutput, calls=%fused_computation.12.clone.1 | convolution fusion | flops 551419904 | bytes 20054020 | tf_op jit(solution)/shard_map/while/body/eval_jaxpr/qhgk,gkhd->qhgd/dot_general | solution.py:32
  292.6 6.9 %fusion.70 = (f32[256,8,8]{0,2,1:T(8,128)S(1)}, f32[256,8,8,256]{0,3,2,1:T(8,128)S(1)}) fusion(f32[8,8,256]{2,1,0:T(8,128)S(1)} %dynamic-slice_bitcast_fusion.4, f32[256,8]{0,1:T(8,128)S(1)} %get-tuple-element.297, bf16[256,8,64]{0,2,1:T(8,128)(2,1)S(1)} %get-tuple-element.296, bf16[2,8,256,8,64]{2,4,1,3,0:T(8,128)(2,1)} %get-tuple-element.295, ...), kind=kOutput, calls=%fused_computation.93.clone.1 | convolution fusion | flops 553631744 | bytes 19800068 | tf_op jit(solution)/shard_map/while/body/eval_jaxpr/qhd,gkhd->qhgk/dot_general | solution.py:25
  299.6 4.8 %fusion.71 = (f32[256,8,8]{0,2,1:T(8,128)S(1)}, f32[256,8]{0,1:T(8,128)S(1)}) fusion(f32[256,8,8,256]{0,3,2,1:T(8,128)S(1)} %get-tuple-element.256, f32[256,8,8]{0,2,1:T(8,128)S(1)} %get-tuple-element.257, pred[256,8,256]{0,2,1:T(8,128)(4,1)S(1)} %broadcast_compare_fusion.6), kind=kLoop, calls=%fused_computation.6.clone.1 | loop fusion | flops 16758784 | bytes 17440768 | tf_op jit(solution)/shard_map/while/body/eval_jaxpr/reduce_sum | solution.py:31
  304.4 0.9 copy-done.2
  305.3 9.5 %fusion.73 = f32[256,8,64]{0,2,1:T(8,128)S(1)} fusion(f32[256,8,8,256]{0,3,2,1:T(8,128)} %copy-done.2, f32[256,8,8]{0,2,1:T(8,128)S(1)} %get-tuple-element.257, pred[256,8,256]{0,2,1:T(8,128)(4,1)S(1)} %broadcast_compare_fusion.6, bf16[2,8,256,8,64]{2,4,1,3,0:T(8,128)(2,1)} %get-tuple-element.299, s32[]{:T(128)S(6)} %copy.62, ...), kind=kOutput, calls=%fused_computation.12.clone.1 | convolution fusion | flops 551419904 | bytes 20054020 | tf_op jit(solution)/shard_map/while/body/eval_jaxpr/qhgk,gkhd->qhgd/dot_general | solution.py:32
  315.2 2.3 all_gather.19
  317.5 3.1 fusion.27
  (75 shorter events, 4.7 us)
Async XLA Ops:
  6.5 19.5 %copy-start = (bf16[512,2048]{1,0:T(8,128)(2,1)S(1)}, bf16[512,2048]{1,0:T(8,128)(2,1)}, u32[]{:S(2)}) copy-start(bf16[512,2048]{1,0:T(8,128)(2,1)} %param.16) | copy-start | bytes 6291460
  6.5 14.1 %all-gather.4.cloned.1.call-start = ((), (), s32[]{:S(2)}) async-start(), calls=%async_computation | async-start | bytes 1572864 | tf_op jit(solution)/shard_map/all_gather | solution.py:73
  7.3 95.4 %all-gather.8.cloned.1.call-start = ((), (), s32[]{:S(2)}) async-start(), calls=%async_computation.2 | async-start | bytes 4456448 | tf_op jit(solution)/shard_map/all_gather | solution.py:125
  22.2 3.6 %copy-start.7 = (f32[64]{0:T(128)S(1)}, f32[64]{0:T(128)}, u32[]{:S(2)}) copy-start(f32[64]{0:T(128)} %param.20) | copy-start | bytes 772
  22.2 3.7 %copy-start.6 = (f32[256,8]{0,1:T(8,128)S(1)}, f32[256,8]{0,1:T(8,128)}, u32[]{:S(2)}) copy-start(f32[256,8]{0,1:T(8,128)} %param.21) | copy-start | bytes 24580
  22.2 3.8 %copy-start.4 = (bf16[256,2048]{1,0:T(8,128)(2,1)S(1)}, bf16[256,2048]{1,0:T(8,128)(2,1)}, u32[]{:S(2)}) copy-start(bf16[256,2048]{1,0:T(8,128)(2,1)} %all-gather.4.cloned.1.call-done) | copy-start | bytes 3145732
  22.2 3.8 %copy-start.10 = (f32[2048]{0:T(1024)S(1)}, f32[2048]{0:T(1024)}, u32[]{:S(2)}) copy-start(f32[2048]{0:T(1024)} %param.14) | copy-start | bytes 24580
  25.7 209.8 %all-gather.6.cloned.1.call-start = ((), (), s32[]{:S(2)}) async-start(), calls=%async_computation.1 | async-start | bytes 11141120 | tf_op jit(solution)/shard_map/all_gather | solution.py:121
  27.8 1.6 copy-start.5
  30.7 6.2 %copy-start.9 = (bf16[512,2048]{1,0:T(8,128)(2,1)S(1)}, bf16[512,2048]{1,0:T(8,128)(2,1)}, u32[]{:S(2)}) copy-start(bf16[512,2048]{1,0:T(8,128)(2,1)} %param.15) | copy-start | bytes 6291460
  33.2 4.5 %copy-start.8 = (f32[64]{0:T(128)S(1)}, f32[64]{0:T(128)}, u32[]{:S(2)}) copy-start(f32[64]{0:T(128)} %param.19) | copy-start | bytes 772
  33.3 5.1 %collective-permute-start = (bf16[16,512]{1,0:T(8,128)(2,1)S(1)}, bf16[16,512]{1,0:T(8,128)(2,1)S(1)}, u32[]{:S(2)}, u32[]{:S(2)}) collective-permute-start(bf16[16,512]{1,0:T(8,128)(2,1)S(1)} %slice.42), channel_id=1, source_target_pairs={{0,2},{2,4},{4,6},{6,8},{8,10},{10,12},{12,14},{14,16},{16,18},{18... | collective-permute-start | bytes 49160 | tf_op jit(solution)/shard_map/ppermute | solution.py:17
  39.6 3.0 copy-start.3
  276.6 5.7 %copy-start.2 = (f32[256,8,8,256]{0,3,2,1:T(8,128)}, f32[256,8,8,256]{0,3,2,1:T(8,128)S(1)}, u32[]{:S(2)}) copy-start(f32[256,8,8,256]{0,3,2,1:T(8,128)S(1)} %get-tuple-element.256) | copy-start | bytes 50331652 | tf_op jit(solution)/shard_map/while
  299.5 5.7 %copy-start.2 = (f32[256,8,8,256]{0,3,2,1:T(8,128)}, f32[256,8,8,256]{0,3,2,1:T(8,128)S(1)}, u32[]{:S(2)}) copy-start(f32[256,8,8,256]{0,3,2,1:T(8,128)S(1)} %get-tuple-element.256) | copy-start | bytes 50331652 | tf_op jit(solution)/shard_map/while
  315.2 5.4 %copy-start.1 = (bf16[512,2048]{1,0:T(8,128)(2,1)S(1)}, bf16[512,2048]{1,0:T(8,128)(2,1)}, u32[]{:S(2)}) copy-start(bf16[512,2048]{1,0:T(8,128)(2,1)} %param.16) | copy-start | bytes 6291460
Sparse Core Ops, SparseCore 0:
  8.9 11.7 all-gather.3
  25.8 76.7 all-gather.7
  105.4 130.0 all-gather.5
